TPU v7x, 32 devices: a whole 2x2x4 slice. The times are simulated.
32 devices in a mesh: sp: 8 (over z, x), tp: 4 (over y, core).
Axes of the slice: x: 2, y: 2, z: 4, core: 2. Of those that a mesh axis runs over, the one named last changes fastest.
Arguments:
- tokens: bfloat16 [2048, 2048], P('sp'), may hold values from -6 to 6
- documents: int32 [2048], P('sp'), may hold values from 0 to 3, never falling along the last dimension, each value on 1 to 1024 neighbouring positions
- norm_gain: float32 [1, 2048], replicated, may hold values from 0.1 to 1.9
- w_query: bfloat16 [1, 2048, 2048], P(None, 'sp', 'tp'), may hold values from -0.125 to 0.125
- w_key: bfloat16 [1, 2048, 2048], P(None, 'sp', 'tp'), may hold values from -0.125 to 0.125
- w_value: bfloat16 [1, 2048, 2048], P(None, 'sp', 'tp'), may hold values from -0.125 to 0.125
- w_out: bfloat16 [1, 2048, 2048], P(None, None, 'sp'), may hold values from -0.59765625 to 0.59765625
- rel_bias: float32 [1, 32, 257], P(None, 'tp'), may hold values from -8 to 240
Outputs:
- mixed: bfloat16 [2048, 2048], P('sp')
Inputs may be any that keep to these rules, and one draw needn't show every extreme that they name: `documents`: document numbers never fall along the sequence; a document has 1 to 1024 positions.
All inputs are finite; a program needn't handle non-finite values.
Results may differ from a plain program's by a relative error of at most 0.007.
Values may be sent and summed in bfloat16 or wider, within the bound.
A program may use at most 128 MiB of HBM per device.

v0:
```python
import jax
import jax.numpy as jnp
from jax import lax
from jax.sharding import PartitionSpec as P

HEAD_DIM = 64
SEG = 64
LEFT = 4
REL_CLIP = 128
EPS = 1e-06


def passed_along(x, axis, by):
    length = lax.axis_size(axis)
    pairs = [(i, i + by) for i in range(length) if 0 <= i + by < length]
    return lax.ppermute(x, axis, pairs)


def banded_bias(bias_table, query_rows, key_rows, reach_rows):
    span_len = query_rows + key_rows - 1
    steps_back = jnp.arange(span_len, dtype=jnp.int32) - (key_rows - 1) + reach_rows
    lookup = jnp.clip(steps_back, -REL_CLIP, REL_CLIP) + REL_CLIP
    bias_line = jnp.take(bias_table, lookup, axis=1)
    reversed_line = bias_line[:, ::-1]
    repeated = jnp.tile(reversed_line, (1, query_rows))
    skewed = repeated[:, query_rows - 1 : query_rows - 1 + query_rows * (span_len - 1)]
    skewed = skewed.reshape(bias_table.shape[0], query_rows, span_len - 1)
    return skewed[:, :, :key_rows]


def attend(queries, keys_all, values_all, query_pos, key_pos, query_doc, key_doc, bias_table):
    query_rows = queries.shape[0]
    key_rows = keys_all.shape[0]
    reach_rows = key_rows - query_rows
    scores = jnp.einsum(
        "qhe,khe->hqk", queries, keys_all, preferred_element_type=jnp.float32
    ) * HEAD_DIM ** (-0.5)
    scores = scores + banded_bias(bias_table, query_rows, key_rows, reach_rows)
    query_seg = query_pos // SEG
    key_seg = key_pos // SEG
    allowed = (
        (key_pos[None, :] >= 0)
        & (key_seg[None, :] <= query_seg[:, None])
        & (key_seg[None, :] >= query_seg[:, None] - LEFT)
        & (key_doc[None, :] == query_doc[:, None])
    )
    scores = jnp.where(allowed[None], scores, -1e30)
    peak = jnp.max(scores, axis=-1, keepdims=True)
    raised = jnp.exp(scores - peak)
    weights_bf = (raised / jnp.sum(raised, axis=-1, keepdims=True)).astype(jnp.bfloat16)
    return jnp.einsum(
        "hqk,khe->qhe", weights_bf, values_all, preferred_element_type=jnp.float32
    ).astype(jnp.bfloat16)


def body(tokens, documents, norm_gain, w_query, w_key, w_value, w_out, rel_bias):
    local_rows = tokens.shape[0]
    reach_rows = LEFT * SEG
    width_local = w_query.shape[2]
    heads_local = width_local // HEAD_DIM
    offset = lax.axis_index("sp") * local_rows
    query_pos = offset + jnp.arange(local_rows, dtype=jnp.int32)
    key_pos = offset - reach_rows + jnp.arange(reach_rows + local_rows, dtype=jnp.int32)
    widened = tokens.astype(jnp.float32)
    normed = (
        widened
        * lax.rsqrt(jnp.mean(widened * widened, axis=-1, keepdims=True) + EPS)
        * norm_gain[0]
    ).astype(jnp.bfloat16)
    query_sum = jnp.dot(
        normed,
        lax.all_gather(w_query[0], "sp", axis=0, tiled=True),
        preferred_element_type=jnp.float32,
    )
    key_sum = jnp.dot(
        normed,
        lax.all_gather(w_key[0], "sp", axis=0, tiled=True),
        preferred_element_type=jnp.float32,
    )
    value_sum = jnp.dot(
        normed,
        lax.all_gather(w_value[0], "sp", axis=0, tiled=True),
        preferred_element_type=jnp.float32,
    )
    queries = query_sum.astype(jnp.bfloat16)
    keys_own = key_sum.astype(jnp.bfloat16)
    values_own = value_sum.astype(jnp.bfloat16)
    prior_keys, prior_values, prior_docs = passed_along((keys_own, values_own, documents), "sp", 1)
    keys_all = jnp.concatenate([prior_keys, keys_own], axis=0)
    values_all = jnp.concatenate([prior_values, values_own], axis=0)
    key_doc = jnp.concatenate([prior_docs, documents], axis=0)
    attended = attend(
        queries.reshape(local_rows, heads_local, HEAD_DIM),
        keys_all.reshape(reach_rows + local_rows, heads_local, HEAD_DIM),
        values_all.reshape(reach_rows + local_rows, heads_local, HEAD_DIM),
        query_pos,
        key_pos,
        documents,
        key_doc,
        rel_bias[0],
    ).reshape(local_rows, width_local)
    all_heads = lax.all_gather(attended, "tp", axis=1, tiled=True)
    return (
        widened
        + jnp.dot(
            all_heads,
            lax.all_gather(w_out[0], "sp", axis=1, tiled=True),
            preferred_element_type=jnp.float32,
        )
    ).astype(jnp.bfloat16)


def solution(mesh):
    in_specs = (
        P("sp", None),
        P("sp"),
        P(),
        P(None, "sp", "tp"),
        P(None, "sp", "tp"),
        P(None, "sp", "tp"),
        P(None, None, "sp"),
        P(None, "tp", None),
    )
    out_specs = P("sp", None)
    return jax.shard_map(body, mesh=mesh, in_specs=in_specs, out_specs=out_specs, check_vma=False)
```

profile of v0, /device:TPU:0, one launch (start us, length us, event | category | flops | bytes accessed | tf_op | source)
XLA Modules:
  0.0 332.9 jit_solution(15047874739899325037)
XLA Ops:
  6.5 0.0 all-gather.12.cloned.1.call-start
  6.5 0.7 all-gather.12.cloned.1.call-update
  7.3 0.0 all-gather.16.cloned.1.call-start
  7.3 0.7 all-gather.16.cloned.1.call-update
  8.0 0.0 all-gather.14.cloned.1.call-start
  8.1 0.7 all-gather.14.cloned.1.call-update
  8.7 0.0 all-gather.10.cloned.1.call-start
  8.8 4.9 %collective-permute-start.1 = (s32[256]{0:T(256)}, s32[256]{0:T(256)S(1)}, u32[]{:S(2)}, u32[]{:S(2)}) collective-permute-start(s32[256]{0:T(256)} %param.9), channel_id=1, source_target_pairs={{0,4},{4,8},{8,12},{12,16},{16,20},{20,24},{24,28},{1,5},{5,9},{9,... | collective-permute-start | bytes 3080 | tf_op jit(solution)/shard_map/ppermute | solution.py:16
  13.7 0.8 copy.17
  14.6 1.6 gather_fusion
  16.2 1.5 fusion.9
  17.7 0.2 select_bitcast_fusion
  17.9 0.5 rev.3
  18.4 0.1 copy.18
  18.5 3.1 tile.4
  21.6 8.7 %tile.10 = f32[8,196352]{1,0:T(8,128)} reshape(f32[8,256,767]{2,1,0:T(8,128)} %tile.4) | data formatting | bytes 12566528 | tf_op jit(solution)/shard_map/tile | solution.py:25
  30.3 5.4 %slice.10 = f32[8,196096]{1,0:T(8,128)} slice(f32[8,196352]{1,0:T(8,128)} %tile.10), slice={[0:8], [255:196351]} | slice | bytes 12550144 | tf_op jit(solution)/shard_map/slice | solution.py:26
  35.7 0.0 copy-start.2
  35.7 12.4 %reshape.203 = f32[8,256,766]{2,1,0:T(8,128)} reshape(f32[8,196096]{1,0:T(8,128)} %slice.10) | data formatting | bytes 12550144 | tf_op jit(solution)/shard_map/reshape | solution.py:27
  48.1 0.0 collective-permute-done.1
  48.1 0.0 copy-done.2
  48.1 0.3 compare_and_fusion
  48.4 12.9 %all-gather.12.cloned.1.call-done = bf16[1,2048,512]{2,1,0:T(8,128)(2,1)} async-done(((bf16[1,256,512]{2,1,0:T(8,128)(2,1)}), bf16[1,2048,512]{2,1,0:T(8,128)(2,1)}) %all-gather.12.cloned.1.call-update) | async-done | bytes 2097168 | tf_op jit(solution)/shard_map/all_gather | solution.py:82
  61.3 0.0 copy-done.1
  61.3 0.0 copy-done.3
  61.3 2.3 fusion.20
  63.7 2.5 collective-permute-start
  66.1 45.1 %all-gather.16.cloned.1.call-done = bf16[1,2048,512]{2,1,0:T(8,128)(2,1)} async-done(((bf16[1,256,512]{2,1,0:T(8,128)(2,1)}), bf16[1,2048,512]{2,1,0:T(8,128)(2,1)}) %all-gather.16.cloned.1.call-update) | async-done | bytes 2097168 | tf_op jit(solution)/shard_map/all_gather | solution.py:77
  111.2 2.3 fusion.26
  113.5 2.7 collective-permute-start.2
  116.3 44.9 %all-gather.14.cloned.1.call-done = bf16[1,2048,512]{2,1,0:T(8,128)(2,1)} async-done(((bf16[1,256,512]{2,1,0:T(8,128)(2,1)}), bf16[1,2048,512]{2,1,0:T(8,128)(2,1)}) %all-gather.14.cloned.1.call-update) | async-done | bytes 2097168 | tf_op jit(solution)/shard_map/all_gather | solution.py:72
  161.1 2.3 fusion.23
  163.5 0.1 copy.15
  163.6 0.0 collective-permute-done
  163.7 0.2 copy.14
  163.9 0.0 collective-permute-done.2
  163.9 0.2 copy.16
  164.1 3.1 fusion.3
  167.2 0.0 copy-start
  167.2 1.7 fusion.41
  169.0 0.2 copy-done
  169.2 8.0 %fusion.19 = bf16[8,64,256]{2,1,0:T(8,128)(2,1)} fusion(bf16[512,8,64]{0,2,1:T(8,128)(2,1)S(1)} %bitcast.41, f32[8,256]{1,0:T(8,128)S(1)} %fusion.41, f32[8,256,512]{2,1,0:T(8,128)} %copy-done), kind=kOutput, calls=%fused_computation.22 | convolution fusion | flops 137497088 | bytes 4988928 | tf_op jit(solution)/shard_map/hqk,khe->qhe/dot_general | solution.py:51
  177.1 0.0 all-gather.10.cloned.1.call-update
  177.1 0.0 all-gather.18.cloned.1.call-start
  177.2 0.5 all-gather.18.cloned.1.call-update
  177.7 14.8 %all-gather.10.cloned.1.call-done = bf16[256,2048]{0,1:T(8,128)(2,1)} async-done(((bf16[256,512]{0,1:T(8,128)(2,1)}), bf16[256,2048]{0,1:T(8,128)(2,1)}) %all-gather.10.cloned.1.call-update) | async-done | bytes 1048592 | tf_op jit(solution)/shard_map/all_gather | solution.py:102
  192.5 126.8 %all-gather.18.cloned.1.call-done = bf16[1,2048,2048]{2,1,0:T(8,128)(2,1)} async-done(((bf16[1,2048,256]{2,1,0:T(8,128)(2,1)}), bf16[1,2048,2048]{2,1,0:T(8,128)(2,1)}) %all-gather.18.cloned.1.call-update) | async-done | bytes 8388624 | tf_op jit(solution)/shard_map/all_gather | solution.py:107
  319.4 7.0 %fusion.6 = bf16[256,2048]{1,0:T(8,128)(2,1)} fusion(bf16[256,2048]{0,1:T(8,128)(2,1)} %all-gather.10.cloned.1.call-done, bf16[1,2048,2048]{2,1,0:T(8,128)(2,1)} %all-gather.18.cloned.1.call-done, bf16[256,2048]{1,0:T(8,128)(2,1)S(1)} %copy-done.1), kind=kOutput, calls=%fused_computation.11 | convolution fusion | flops 2149056512 | bytes 11534336 | tf_op jit(solution)/shard_map/dot_general | solution.py:105
  (12 shorter events, 0.2 us)
Async XLA Ops:
  6.5 54.8 %all-gather.12.cloned.1.call-start = ((), (), s32[]{:S(2)}) async-start(), calls=%async_computation.1 | async-start | bytes 2359296 | tf_op jit(solution)/shard_map/all_gather | solution.py:82
  7.3 103.9 %all-gather.16.cloned.1.call-start = ((), (), s32[]{:S(2)}) async-start(), calls=%async_computation.3 | async-start | bytes 2359296 | tf_op jit(solution)/shard_map/all_gather | solution.py:77
  8.0 153.1 %all-gather.14.cloned.1.call-start = ((), (), s32[]{:S(2)}) async-start(), calls=%async_computation.2 | async-start | bytes 2359296 | tf_op jit(solution)/shard_map/all_gather | solution.py:72
  8.7 183.8 %all-gather.10.cloned.1.call-start = ((), (), s32[]{:S(2)}) async-start(), calls=%async_computation | async-start | bytes 1310720 | tf_op jit(solution)/shard_map/all_gather | solution.py:102
  8.8 39.3 %collective-permute-start.1 = (s32[256]{0:T(256)}, s32[256]{0:T(256)S(1)}, u32[]{:S(2)}, u32[]{:S(2)}) collective-permute-start(s32[256]{0:T(256)} %param.9), channel_id=1, source_target_pairs={{0,4},{4,8},{8,12},{12,16},{16,20},{20,24},{24,28},{1,5},{5,9},{9,... | collective-permute-start | bytes 3080 | tf_op jit(solution)/shard_map/ppermute | solution.py:16
  35.7 12.4 %copy-start.2 = (s32[256]{0:T(256)S(1)}, s32[256]{0:T(256)}, u32[]{:S(2)}) copy-start(s32[256]{0:T(256)} %param.9) | copy-start | bytes 3076
  35.7 25.6 %copy-start.1 = (bf16[256,2048]{1,0:T(8,128)(2,1)S(1)}, bf16[256,2048]{1,0:T(8,128)(2,1)}, u32[]{:S(2)}) copy-start(bf16[256,2048]{1,0:T(8,128)(2,1)} %param.8) | copy-start | bytes 3145732
  35.7 25.6 %copy-start.3 = (f32[1,2048]{1,0:T(1,128)S(1)}, f32[1,2048]{1,0:T(1,128)}, u32[]{:S(2)}) copy-start(f32[1,2048]{1,0:T(1,128)} %param.10) | copy-start | bytes 24580
  63.7 100.0 %collective-permute-start = (bf16[256,512]{1,0:T(8,128)(2,1)S(1)}, bf16[256,512]{1,0:T(8,128)(2,1)S(1)}, u32[]{:S(2)}, u32[]{:S(2)}) collective-permute-start(bf16[256,512]{1,0:T(8,128)(2,1)S(1)} %fusion.20), channel_id=1, source_target_pairs={{0,4},{4,8},{8,12},{12,16},{16,20},{20,24},{24,28},{1,5},{5,9},{9,... | collective-permute-start | bytes 786440 | tf_op jit(solution)/shard_map/ppermute | solution.py:16
  113.5 50.3 %collective-permute-start.2 = (bf16[256,512]{1,0:T(8,128)(2,1)S(1)}, bf16[256,512]{1,0:T(8,128)(2,1)S(1)}, u32[]{:S(2)}, u32[]{:S(2)}) collective-permute-start(bf16[256,512]{1,0:T(8,128)(2,1)S(1)} %fusion.26), channel_id=1, source_target_pairs={{0,4},{4,8},{8,12},{12,16},{16,20},{20,24},{24,28},{1,5},{5,9},{9,... | collective-permute-start | bytes 786440 | tf_op jit(solution)/shard_map/ppermute | solution.py:16
  167.2 1.9 copy-start
  177.1 142.2 %all-gather.18.cloned.1.call-start = ((), (), s32[]{:S(2)}) async-start(), calls=%async_computation.4 | async-start | bytes 9437184 | tf_op jit(solution)/shard_map/all_gather | solution.py:107
Sparse Core Ops, SparseCore 0:
  9.5 51.7 all-gather.11
  63.4 47.7 all-gather.15
  113.3 47.7 all-gather.13
  177.3 15.2 all-gather.9
  194.4 124.9 all-gather.17
where the time goes:
time: 333 us
  waiting for transfers between devices  247 us (74%)
  local copies, waits for them, and re-layouts  33.3 us (10%)
  matrix products  25.1 us (8%)
  between operations  13.3 us (4%)
  starting transfers between devices  10.2 us (3%)
  other arithmetic  3.84 us (1%)
    all_gather x1, waiting for transfers between devices, body(): lax.all_gather(w_out[0], 'sp', axis=1, tiled=True)  127 us
    all_gather x1, waiting for transfers between devices, body(): lax.all_gather(w_key[0], 'sp', axis=0, tiled=True)  45.1 us
    all_gather x1, waiting for transfers between devices, body(): lax.all_gather(w_query[0], 'sp', axis=0, tiled=True)  44.9 us
    all_gather x1, waiting for transfers between devices, body(): all_heads = lax.all_gather(attended, 'tp', axis=1, tiled=True)  14.8 us
    all_gather x1, waiting for transfers between devices, body(): lax.all_gather(w_value[0], 'sp', axis=0, tiled=True)  12.9 us
    reshape x1, local copies, waits for them, and re-layouts, banded_bias(): skewed = skewed.reshape(bias_table.shape[0], query_rows, span_len - 1)  12.4 us
    another operation x2, local copies, waits for them, and re-layouts, banded_bias(): repeated = jnp.tile(reversed_line, (1, query_rows))  11.8 us
    ppermute x3, starting transfers between devices, passed_along(): return lax.ppermute(x, axis, pairs)  10 us
  transfers between devices with their start and end apart: 8, of which 5 were waited for; matrix products, arithmetic and copies ran while one was open for 13% of the time, Pallas kernels for 0%

commit v1 on v0

--- a/solution.py
+++ b/solution.py
@@ -69,7 +69,9 @@
     ).astype(jnp.bfloat16)
     query_sum = jnp.dot(
         normed,
-        lax.all_gather(w_query[0], "sp", axis=0, tiled=True),
+        jnp.concatenate(
+            lax.all_to_all(jnp.stack([w_query[0]] * lax.axis_size("sp")), "sp", 0, 0), axis=0
+        ),
         preferred_element_type=jnp.float32,
     )
     key_sum = jnp.dot(

time: 333 us -> 327 us (0.982)
  waiting for transfers between devices: 247 us -> 225 us
  starting transfers between devices: 10.2 us -> 17.2 us
  local copies, waits for them, and re-layouts: 33.3 us -> 38.3 us
  other arithmetic: 3.84 us -> 7.44 us
    all_gather x1 -> x0, waiting for transfers between devices: 44.9 us -> none  [body(): lax.all_gather(w_query[0], 'sp', axis=0, tiled=True)]
    all_gather x1, waiting for transfers between devices: 12.9 us -> 31.9 us  [body(): lax.all_gather(w_value[0], 'sp', axis=0, tiled=True)]
    all_to_all x0 -> x1, starting transfers between devices: none -> 7.41 us  [body(): lax.all_to_all(jnp.stack([w_query[0]] * lax.axis_size('sp')), 'sp', 0, 0)]
    all_gather x1, waiting for transfers between devices: 14.8 us -> 18.7 us  [body(): all_heads = lax.all_gather(attended, 'tp', axis=1, tiled=True)]
  transfers between devices with their start and end apart: 8 -> 8, of which waited for: 5 -> 5; matrix products, arithmetic and copies ran while one was open for 13% -> 15% of each run, Pallas kernels for 0% -> 0%
where the time goes in v1:
time: 327 us; the launch traced here: 326 us
  waiting for transfers between devices  225 us (69%)
  local copies, waits for them, and re-layouts  38.3 us (12%)
  matrix products  24.9 us (8%)
  starting transfers between devices  17.2 us (5%)
  between operations  13.3 us (4%)
  other arithmetic  7.44 us (2%)
    all_gather x1, waiting for transfers between devices, body(): lax.all_gather(w_out[0], 'sp', axis=1, tiled=True)  127 us
    all_gather x1, waiting for transfers between devices, body(): lax.all_gather(w_key[0], 'sp', axis=0, tiled=True)  44.3 us
    all_gather x1, waiting for transfers between devices, body(): lax.all_gather(w_value[0], 'sp', axis=0, tiled=True)  31.9 us
    all_gather x1, waiting for transfers between devices, body(): all_heads = lax.all_gather(attended, 'tp', axis=1, tiled=True)  18.7 us
    reshape x1, local copies, waits for them, and re-layouts, banded_bias(): skewed = skewed.reshape(bias_table.shape[0], query_rows, span_len - 1)  12.3 us
    another operation x2, local copies, waits for them, and re-layouts, banded_bias(): repeated = jnp.tile(reversed_line, (1, query_rows))  11.8 us
    ppermute x3, starting transfers between devices, passed_along(): return lax.ppermute(x, axis, pairs)  9.7 us
    dot_general x1, matrix products, attend(): jnp.einsum('hqk,khe->qhe', weights_bf, values_all, preferred_element_type...  7.95 us
  transfers between devices with their start and end apart: 8, of which 5 were waited for; matrix products, arithmetic and copies ran while one was open for 15% of the time, Pallas kernels for 0%

profile of v1, /device:TPU:0, one launch (start us, length us, event | category | flops | bytes accessed | tf_op | source)
XLA Modules:
  0.0 326.1 jit_solution(3843189563401212288)
XLA Ops:
  6.5 0.7 all-gather.10.cloned.1.call-update
  7.3 0.0 all-gather.12.cloned.1.call-start
  7.3 0.7 all-gather.12.cloned.1.call-update
  8.0 2.5 stack.3
  10.5 7.4 %all-to-all-start = ((bf16[8,256,512]{2,1,0:T(8,128)(2,1)}), bf16[8,256,512]{2,1,0:T(8,128)(2,1)S(1)}, u32[]{:S(2)}, u32[]{:S(2)}) async-start(bf16[8,256,512]{2,1,0:T(8,128)(2,1)} %stack.3), calls=%async_computation | async-start | bytes 4194304 | tf_op jit(solution)/shard_map/all_to_all | solution.py:73
  17.9 0.0 all-gather.8.cloned.1.call-start
  17.9 4.4 %collective-permute-start.1 = (s32[256]{0:T(256)S(1)}, s32[256]{0:T(256)}, u32[]{:S(2)}, u32[]{:S(2)}) collective-permute-start(s32[256]{0:T(256)S(1)} %copy-done.3), channel_id=1, source_target_pairs={{0,4},{4,8},{8,12},{12,16},{16,20},{20,24},{24,28},{1,5},{5,9},{9,... | collective-permute-start | bytes 3080 | tf_op jit(solution)/shard_map/ppermute | solution.py:16
  22.4 0.1 copy.17
  22.5 2.3 gather_fusion
  24.9 0.3 fusion.9
  25.2 0.6 add_rsqrt_fusion
  25.8 1.2 select_bitcast_fusion
  26.9 0.5 fusion.30
  27.5 2.0 rev.3
  29.5 1.1 copy.18
  30.6 3.1 tile.4
  33.7 8.7 %tile.10 = f32[8,196352]{1,0:T(8,128)} reshape(f32[8,256,767]{2,1,0:T(8,128)} %tile.4) | data formatting | bytes 12566528 | tf_op jit(solution)/shard_map/tile | solution.py:25
  42.4 5.4 %slice.10 = f32[8,196096]{1,0:T(8,128)} slice(f32[8,196352]{1,0:T(8,128)} %tile.10), slice={[0:8], [255:196351]} | slice | bytes 12550144 | tf_op jit(solution)/shard_map/slice | solution.py:26
  47.8 12.3 %reshape.208 = f32[8,256,766]{2,1,0:T(8,128)} reshape(f32[8,196096]{1,0:T(8,128)} %slice.10) | data formatting | bytes 12550144 | tf_op jit(solution)/shard_map/reshape | solution.py:27
  60.1 0.0 collective-permute-done.1
  60.1 0.6 pad_add_fusion
  60.8 0.3 compare_and_fusion
  61.0 31.9 %all-gather.10.cloned.1.call-done = bf16[1,2048,512]{2,1,0:T(8,128)(2,1)} async-done(((bf16[1,256,512]{2,1,0:T(8,128)(2,1)}), bf16[1,2048,512]{2,1,0:T(8,128)(2,1)}) %all-gather.10.cloned.1.call-update) | async-done | bytes 2097168 | tf_op jit(solution)/shard_map/all_gather | solution.py:84
  93.0 0.0 copy-done.7
  93.0 3.0 fusion.18
  96.0 2.1 collective-permute-start
  98.1 44.3 %all-gather.12.cloned.1.call-done = bf16[1,2048,512]{2,1,0:T(8,128)(2,1)} async-done(((bf16[1,256,512]{2,1,0:T(8,128)(2,1)}), bf16[1,2048,512]{2,1,0:T(8,128)(2,1)}) %all-gather.12.cloned.1.call-update) | async-done | bytes 2097168 | tf_op jit(solution)/shard_map/all_gather | solution.py:79
  142.4 3.1 fusion.21
  145.5 3.2 collective-permute-start.2
  148.6 0.0 all-to-all-done
  148.6 0.8 convolution_convert_fusion
  149.4 0.1 copy.15
  149.5 0.0 collective-permute-done
  149.6 1.1 pad_maximum_fusion
  150.6 0.2 copy.14
  150.8 1.3 collective-permute-done.2
  152.1 1.1 pad_maximum_fusion.1
  153.2 0.2 copy.16
  153.4 3.1 fusion.3
  156.5 1.7 fusion.36
  158.2 0.2 copy-done
  158.4 8.0 %fusion.17 = bf16[8,64,256]{2,1,0:T(8,128)(2,1)} fusion(bf16[512,8,64]{0,2,1:T(8,128)(2,1)S(1)} %bitcast.40, f32[8,256]{1,0:T(8,128)S(1)} %fusion.36, f32[8,256,512]{2,1,0:T(8,128)} %copy-done), kind=kOutput, calls=%fused_computation.20 | convolution fusion | flops 137497088 | bytes 4988928 | tf_op jit(solution)/shard_map/hqk,khe->qhe/dot_general | solution.py:51
  166.4 0.0 all-gather.8.cloned.1.call-update
  166.4 0.0 all-gather.14.cloned.1.call-start
  166.4 0.5 all-gather.14.cloned.1.call-update
  167.0 18.7 %all-gather.8.cloned.1.call-done = bf16[256,2048]{0,1:T(8,128)(2,1)} async-done(((bf16[256,512]{0,1:T(8,128)(2,1)}), bf16[256,2048]{0,1:T(8,128)(2,1)}) %all-gather.8.cloned.1.call-update) | async-done | bytes 1048592 | tf_op jit(solution)/shard_map/all_gather | solution.py:104
  185.7 126.9 %all-gather.14.cloned.1.call-done = bf16[1,2048,2048]{2,1,0:T(8,128)(2,1)} async-done(((bf16[1,2048,256]{2,1,0:T(8,128)(2,1)}), bf16[1,2048,2048]{2,1,0:T(8,128)(2,1)}) %all-gather.14.cloned.1.call-update) | async-done | bytes 8388624 | tf_op jit(solution)/shard_map/all_gather | solution.py:109
  312.6 7.0 %fusion.6 = bf16[256,2048]{1,0:T(8,128)(2,1)} fusion(bf16[256,2048]{0,1:T(8,128)(2,1)} %all-gather.8.cloned.1.call-done, bf16[1,2048,2048]{2,1,0:T(8,128)(2,1)} %all-gather.14.cloned.1.call-done, bf16[256,2048]{1,0:T(8,128)(2,1)S(1)} %copy-done.1), kind=kOutput, calls=%fused_computation.11 | convolution fusion | flops 2149056512 | bytes 11534336 | tf_op jit(solution)/shard_map/dot_general | solution.py:107
  (22 shorter events, 0.1 us)
Async XLA Ops:
  6.5 86.4 %all-gather.10.cloned.1.call-start = ((), (), s32[]{:S(2)}) async-start(), calls=%async_computation.2 | async-start | bytes 2359296 | tf_op jit(solution)/shard_map/all_gather | solution.py:84
  7.3 135.2 %all-gather.12.cloned.1.call-start = ((), (), s32[]{:S(2)}) async-start(), calls=%async_computation.3 | async-start | bytes 2359296 | tf_op jit(solution)/shard_map/all_gather | solution.py:79
  10.5 7.5 %copy-start.3 = (s32[256]{0:T(256)S(1)}, s32[256]{0:T(256)}, u32[]{:S(2)}) copy-start(s32[256]{0:T(256)} %param.9) | copy-start | bytes 3076
  10.5 11.9 %copy-start.2 = (f32[1,8,257]{2,1,0:T(8,128)S(1)}, f32[1,8,257]{2,1,0:T(8,128)}, u32[]{:S(2)}) copy-start(f32[1,8,257]{2,1,0:T(8,128)} %param.15) | copy-start | bytes 24676
  10.5 14.4 %copy-start.1 = (bf16[256,2048]{1,0:T(8,128)(2,1)S(1)}, bf16[256,2048]{1,0:T(8,128)(2,1)}, u32[]{:S(2)}) copy-start(bf16[256,2048]{1,0:T(8,128)(2,1)} %param.8) | copy-start | bytes 3145732
  10.5 138.2 %all-to-all-start = ((bf16[8,256,512]{2,1,0:T(8,128)(2,1)}), bf16[8,256,512]{2,1,0:T(8,128)(2,1)S(1)}, u32[]{:S(2)}, u32[]{:S(2)}) async-start(bf16[8,256,512]{2,1,0:T(8,128)(2,1)} %stack.3), calls=%async_computation | async-start | bytes 4194304 | tf_op jit(solution)/shard_map/all_to_all | solution.py:73
  17.9 167.8 %all-gather.8.cloned.1.call-start = ((), (), s32[]{:S(2)}) async-start(), calls=%async_computation.1 | async-start | bytes 1310720 | tf_op jit(solution)/shard_map/all_gather | solution.py:104
  17.9 42.2 %collective-permute-start.1 = (s32[256]{0:T(256)S(1)}, s32[256]{0:T(256)}, u32[]{:S(2)}, u32[]{:S(2)}) collective-permute-start(s32[256]{0:T(256)S(1)} %copy-done.3), channel_id=1, source_target_pairs={{0,4},{4,8},{8,12},{12,16},{16,20},{20,24},{24,28},{1,5},{5,9},{9,... | collective-permute-start | bytes 3080 | tf_op jit(solution)/shard_map/ppermute | solution.py:16
  47.8 13.0 %copy-start.6 = (pred[512]{0:T(512)(128)(4,1)S(1)}, pred[512]{0:T(512)(128)(4,1)}, u32[]{:S(2)}) copy-start(pred[512]{0:T(512)(128)(4,1)} %fusion.30) | copy-start | bytes 1540
  47.8 45.2 %copy-start.4 = (f32[256]{0:T(256)S(1)}, f32[256]{0:T(256)}, u32[]{:S(2)}) copy-start(f32[256]{0:T(256)} %add_rsqrt_fusion) | copy-start | bytes 3076
  47.8 45.2 %copy-start.7 = (f32[1,2048]{1,0:T(1,128)S(1)}, f32[1,2048]{1,0:T(1,128)}, u32[]{:S(2)}) copy-start(f32[1,2048]{1,0:T(1,128)} %param.10) | copy-start | bytes 24580
  96.0 52.6 %copy-start.5 = (f32[256]{0:T(256)S(1)}, f32[256]{0:T(256)}, u32[]{:S(2)}) copy-start(f32[256]{0:T(256)} %add_rsqrt_fusion) | copy-start | bytes 3076
  96.0 52.6 %copy-start.8 = (f32[1,2048]{1,0:T(1,128)S(1)}, f32[1,2048]{1,0:T(1,128)}, u32[]{:S(2)}) copy-start(f32[1,2048]{1,0:T(1,128)} %param.10) | copy-start | bytes 24580
  96.0 53.5 %collective-permute-start = (bf16[256,512]{1,0:T(8,128)(2,1)}, bf16[256,512]{1,0:T(8,128)(2,1)}, u32[]{:S(2)}, u32[]{:S(2)}) collective-permute-start(bf16[256,512]{1,0:T(8,128)(2,1)} %fusion.18), channel_id=1, source_target_pairs={{0,4},{4,8},{8,12},{12,16},{16,20},{20,24},{24,28},{1,5},{5,9},{9,... | collective-permute-start | bytes 786440 | tf_op jit(solution)/shard_map/ppermute | solution.py:16
  145.5 6.6 %collective-permute-start.2 = (bf16[256,512]{1,0:T(8,128)(2,1)}, bf16[256,512]{1,0:T(8,128)(2,1)}, u32[]{:S(2)}, u32[]{:S(2)}) collective-permute-start(bf16[256,512]{1,0:T(8,128)(2,1)} %fusion.21), channel_id=1, source_target_pairs={{0,4},{4,8},{8,12},{12,16},{16,20},{20,24},{24,28},{1,5},{5,9},{9,... | collective-permute-start | bytes 786440 | tf_op jit(solution)/shard_map/ppermute | solution.py:16
  156.5 2.0 copy-start
  166.4 146.2 %all-gather.14.cloned.1.call-start = ((), (), s32[]{:S(2)}) async-start(), calls=%async_computation.4 | async-start | bytes 9437184 | tf_op jit(solution)/shard_map/all_gather | solution.py:109
Sparse Core Ops, SparseCore 0:
  9.5 83.4 all-gather.9
  95.1 47.2 all-gather.11
  166.5 19.1 all-gather.7
  187.6 124.9 all-gather.13
